TPU v7x, 32 devices: a whole 2x2x4 slice. The times are simulated.
32 devices in a mesh: ra: 2 (over core), cb: 4 (over z), dp: 4 (over y, x).
Axes of the slice: x: 2, y: 2, z: 4, core: 2. Of those that a mesh axis runs over, the one named last changes fastest.
Arguments:
- residual_in: bfloat16 [1024, 4096], P('dp', 'cb'), may hold values from -220 to 220, as said below
- gain_in: float32 [4096], P('cb'), may hold values from 0.1 to 1.9
- shift_in: float32 [4096], P('cb'), may hold values from -3 to 3
- up_weight: bfloat16 [4096, 16384], P('cb', 'ra'), may hold values from -0.09375 to 0.09375
- down_weight: bfloat16 [16384, 4096], P('ra', 'cb'), may hold values from -0.046875 to 0.046875
- gain_out: float32 [4096], P('cb'), may hold values from 0.1 to 1.9
- shift_out: float32 [4096], P('cb'), may hold values from -3 to 3
Outputs:
- layer_out: bfloat16 [1024, 4096], P('dp', 'cb')
Inputs may be any that keep to these rules, and one draw needn't show every extreme that they name: `residual_in`: real-valued activations.
All inputs are finite; a program needn't handle non-finite values.
Results may differ from a plain program's by a relative error of at most 0.0065.
Values may be sent and summed in bfloat16 or wider, within the bound.
No kernel may reach another device: no remote copies, remote signals or barrier semaphores. Data moves between devices by JAX's collectives and lax.ppermute only.
A program may use at most 128 MiB of HBM per device.

v0:
```python
import jax
import jax.numpy as jnp
from jax import lax
from jax.sharding import PartitionSpec as P


def standardize(values):
    count = values.shape[1] * lax.axis_size("cb")
    sums = lax.psum(jnp.sum(values, axis=1), "cb")
    mean = sums / count
    centred = values - mean[:, None]
    spread = lax.psum(jnp.sum(centred * centred, axis=1), "cb") / count
    return (values - mean[:, None]) * lax.rsqrt(spread + 1e-05)[:, None]


def per_device(residual_in, gain_in, shift_in, up_weight, down_weight, gain_out, shift_out):
    normed = (standardize(residual_in.astype(jnp.float32)) * gain_in + shift_in).astype(
        jnp.bfloat16
    )
    products = jnp.dot(normed, up_weight, preferred_element_type=jnp.float32)
    share = lax.psum_scatter(products, "cb", scatter_dimension=1, tiled=True)
    hidden_share = jnp.square(jax.nn.relu(share)).astype(jnp.bfloat16)
    branch_part = jnp.dot(
        lax.all_gather(hidden_share, "cb", axis=1, tiled=True),
        down_weight,
        preferred_element_type=jnp.float32,
    )
    branch = lax.psum(branch_part, "ra")
    total = 2.0**0.25 * normed.astype(jnp.float32) + branch
    return (standardize(total) * gain_out + shift_out).astype(jnp.bfloat16)


def solution(mesh):
    in_specs = (P("dp", "cb"), P("cb"), P("cb"), P("cb", "ra"), P("ra", "cb"), P("cb"), P("cb"))
    out_specs = P("dp", "cb")
    return jax.shard_map(
        per_device, mesh=mesh, in_specs=in_specs, out_specs=out_specs, check_vma=False
    )
```

profile of v0, /device:TPU:0, one launch (start us, length us, event | category | flops | bytes accessed | tf_op | source)
XLA Modules:
  0.0 337.2 jit_solution(11542523909155165681)
XLA Ops:
  6.5 0.0 reduce-scatter.2.cloned.1.call-start
  6.5 1.2 convert_reduce_fusion
  7.7 13.5 %psum.35 = f32[256]{0:T(256)S(1)} all-reduce(f32[256]{0:T(256)S(1)} %convert_reduce_fusion), channel_id=1, replica_groups=mesh['ra'=2,'cb'=4,'dp'=4] {'cb'}, use_global_device_ids=true, to_apply=%region_1.0 | all-reduce | flops 256 | bytes 2048 | tf_op jit(solution)/shard_map/psum | solution.py:9
  21.2 1.3 fusion.2
  22.5 8.4 %psum.36 = f32[256]{0:T(256)S(1)} all-reduce(f32[256]{0:T(256)S(1)} %fusion.2), channel_id=1, replica_groups=mesh['ra'=2,'cb'=4,'dp'=4] {'cb'}, use_global_device_ids=true, to_apply=%region_3.0 | all-reduce | flops 256 | bytes 2048 | tf_op jit(solution)/shard_map/psum | solution.py:12
  30.9 13.8 %fusion.7 = f32[256,8192]{1,0:T(8,128)} fusion(bf16[1024,8192]{1,0:T(8,128)(2,1)} %param.10, bf16[256,1024]{1,0:T(8,128)(2,1)} %param.7, f32[1024]{0:T(1024)} %param.9, f32[1024]{0:T(1024)} %param.8, f32[256]{0:T(256)S(1)} %add_rsqrt_fusion.1, f32[256]{0:T(256)S(1)} %broadcast_multiply_fusion.1), kind=kOutput, calls=%fused_computation.17 | convolution fusion | flops 4296540160 | bytes 25700352 | tf_op jit(solution)/shard_map/dot_general | solution.py:20
  44.8 0.0 reduce-scatter.2.cloned.1.call-update
  44.8 0.0 all-gather.2.cloned.1.call-start
  44.8 144.4 %reduce-scatter.2.cloned.1.call-done = f32[256,2048]{1,0:T(8,128)} async-done(((f32[256,8192]{1,0:T(8,128)}), f32[256,2048]{1,0:T(8,128)}) %reduce-scatter.2.cloned.1.call-update) | async-done | bytes 2097168 | tf_op jit(solution)/shard_map/reduce_scatter | solution.py:21
  189.2 2.8 multiply_convert_fusion
  192.0 0.0 all-gather.2.cloned.1.call-update
  192.0 0.0 copy-start
  192.0 0.0 copy-start.1
  192.1 0.0 copy-start.2
  192.1 0.0 copy-start.3
  192.1 0.0 copy-start.4
  192.1 0.0 all-reduce.2.cloned.1.call-start
  192.1 81.4 %all-gather.2.cloned.1.call-done = bf16[256,8192]{1,0:T(8,128)(2,1)} async-done(((bf16[256,2048]{1,0:T(8,128)(2,1)}), bf16[256,8192]{1,0:T(8,128)(2,1)}) %all-gather.2.cloned.1.call-update) | async-done | bytes 4194320 | tf_op jit(solution)/shard_map/all_gather | solution.py:24
  273.5 12.5 %fusion.9 = f32[256,1024]{1,0:T(8,128)} fusion(bf16[256,8192]{1,0:T(8,128)(2,1)} %all-gather.2.cloned.1.call-done, bf16[8192,1024]{1,0:T(8,128)(2,1)} %param.11), kind=kOutput, calls=%fused_computation.18 | convolution fusion | flops 4294967296 | bytes 22020096 | tf_op jit(solution)/shard_map/dot_general | solution.py:23
  286.0 0.0 all-reduce.2.cloned.1.call-update
  286.1 18.1 %all-reduce.2.cloned.1.call-done = f32[256,1024]{1,0:T(8,128)} async-done(((f32[256,1024]{1,0:T(8,128)}), f32[256,1024]{1,0:T(8,128)}) %all-reduce.2.cloned.1.call-update) | async-done | bytes 1048592 | tf_op jit(solution)/shard_map/psum | solution.py:28
  304.1 0.0 copy-done
  304.1 0.0 copy-done.1
  304.1 0.0 copy-done.2
  304.1 1.7 fusion.6
  305.8 12.0 %psum.38 = f32[256]{0:T(256)S(1)} all-reduce(f32[256]{0:T(256)S(1)} %fusion.6), channel_id=1, replica_groups=mesh['ra'=2,'cb'=4,'dp'=4] {'cb'}, use_global_device_ids=true, to_apply=%region_7.8 | all-reduce | flops 256 | bytes 2048 | tf_op jit(solution)/shard_map/psum | solution.py:9
  317.8 1.7 multiply_reduce_fusion
  319.5 8.4 %psum.39 = f32[256]{0:T(256)S(1)} all-reduce(f32[256]{0:T(256)S(1)} %multiply_reduce_fusion), channel_id=1, replica_groups=mesh['ra'=2,'cb'=4,'dp'=4] {'cb'}, use_global_device_ids=true, to_apply=%region_9.10 | all-reduce | flops 256 | bytes 2048 | tf_op jit(solution)/shard_map/psum | solution.py:12
  327.9 0.0 copy-done.3
  327.9 0.0 copy-done.4
  327.9 2.8 add_convert_fusion
  (4 shorter events, 0.0 us)
Async XLA Ops:
  6.5 182.7 %reduce-scatter.2.cloned.1.call-start = ((), (), s32[]{:S(2)}) async-start(), calls=%async_computation.1 | async-start | bytes 10485760 | tf_op jit(solution)/shard_map/reduce_scatter | solution.py:21
  44.8 228.8 %all-gather.2.cloned.1.call-start = ((), (), s32[]{:S(2)}) async-start(), calls=%async_computation.2 | async-start | bytes 5242880 | tf_op jit(solution)/shard_map/all_gather | solution.py:24
  192.0 112.1 %copy-start = (bf16[256,1024]{1,0:T(8,128)(2,1)S(1)}, bf16[256,1024]{1,0:T(8,128)(2,1)}, u32[]{:S(2)}) copy-start(bf16[256,1024]{1,0:T(8,128)(2,1)} %param.7) | copy-start | bytes 1572868
  192.0 112.1 %copy-start.1 = (f32[1024]{0:T(1024)S(1)}, f32[1024]{0:T(1024)}, u32[]{:S(2)}) copy-start(f32[1024]{0:T(1024)} %param.9) | copy-start | bytes 12292
  192.1 112.1 %copy-start.2 = (f32[1024]{0:T(1024)S(1)}, f32[1024]{0:T(1024)}, u32[]{:S(2)}) copy-start(f32[1024]{0:T(1024)} %param.8) | copy-start | bytes 12292
  192.1 135.8 %copy-start.3 = (f32[1024]{0:T(1024)S(1)}, f32[1024]{0:T(1024)}, u32[]{:S(2)}) copy-start(f32[1024]{0:T(1024)} %param.13) | copy-start | bytes 12292
  192.1 135.8 %copy-start.4 = (f32[1024]{0:T(1024)S(1)}, f32[1024]{0:T(1024)}, u32[]{:S(2)}) copy-start(f32[1024]{0:T(1024)} %param.12) | copy-start | bytes 12292
  192.1 112.0 %all-reduce.2.cloned.1.call-start = ((), (), s32[]{:S(2)}) async-start(), calls=%async_computation.3 | async-start | bytes 2097152 | tf_op jit(solution)/shard_map/psum | solution.py:28
Sparse Core Ops, SparseCore 0:
  44.9 144.2 reduce-scatter.1
  192.2 81.3 all-gather.1
  286.2 17.8 all-reduce.1
where the time goes:
time: 338 us; the launch traced here: 337 us
  waiting for transfers between devices  244 us (72%)
  blocking collectives  42.2 us (12%)
  matrix products  26.3 us (8%)
  between operations  13.2 us (4%)
  other arithmetic  11.5 us (3%)
    reduce_scatter x1, waiting for transfers between devices, per_device(): share = lax.psum_scatter(products, 'cb', scatter_dimension=1, tiled=True)  144 us
    all_gather x1, waiting for transfers between devices, per_device(): lax.all_gather(hidden_share, 'cb', axis=1, tiled=True)  81.4 us
    psum x2, blocking collectives, standardize(): sums = lax.psum(jnp.sum(values, axis=1), 'cb')  25.5 us
    psum x1, waiting for transfers between devices, per_device(): branch = lax.psum(branch_part, 'ra')  18.1 us
    psum x2, blocking collectives, standardize(): spread = lax.psum(jnp.sum(centred * centred, axis=1), 'cb') / count  16.7 us
    dot_general x1, matrix products, per_device(): products = jnp.dot(normed, up_weight, preferred_element_type=jnp.float32)  13.8 us
    dot_general x1, matrix products, per_device(): jnp.dot(lax.all_gather(hidden_share, 'cb', axis=1, tiled=True), down_weig...  12.5 us
  transfers between devices with their start and end apart: 3, of which 3 were waited for; matrix products, arithmetic and copies ran while one was open for 0% of the time, Pallas kernels for 0%

commit v1 on v0

--- a/solution.py
+++ b/solution.py
@@ -25,7 +25,7 @@
         down_weight,
         preferred_element_type=jnp.float32,
     )
-    branch = lax.psum(branch_part, "ra")
+    branch = jnp.sum(lax.all_gather(branch_part, "ra"), axis=0)
     total = 2.0**0.25 * normed.astype(jnp.float32) + branch
     return (standardize(total) * gain_out + shift_out).astype(jnp.bfloat16)
 

time: 338 us -> 327 us (0.967)
  waiting for transfers between devices: 244 us -> 235 us
    psum x1 -> x0, waiting for transfers between devices: 18.1 us -> none  [per_device(): branch = lax.psum(branch_part, 'ra')]
    all_gather x0 -> x1, waiting for transfers between devices: none -> 9.22 us  [per_device(): branch = jnp.sum(lax.all_gather(branch_part, 'ra'), axis=0)]
where the time goes in v1:
time: 327 us
  waiting for transfers between devices  235 us (72%)
  blocking collectives  42.2 us (13%)
  matrix products  26.3 us (8%)
  between operations  13.2 us (4%)
  other arithmetic  9.8 us (3%)
    reduce_scatter x1, waiting for transfers between devices, per_device(): share = lax.psum_scatter(products, 'cb', scatter_dimension=1, tiled=True)  144 us
    all_gather x1, waiting for transfers between devices, per_device(): lax.all_gather(hidden_share, 'cb', axis=1, tiled=True)  81.4 us
    psum x2, blocking collectives, standardize(): sums = lax.psum(jnp.sum(values, axis=1), 'cb')  25.4 us
    psum x2, blocking collectives, standardize(): spread = lax.psum(jnp.sum(centred * centred, axis=1), 'cb') / count  16.7 us
    dot_general x1, matrix products, per_device(): products = jnp.dot(normed, up_weight, preferred_element_type=jnp.float32)  13.8 us
    dot_general x1, matrix products, per_device(): jnp.dot(lax.all_gather(hidden_share, 'cb', axis=1, tiled=True), down_weig...  12.5 us
    all_gather x1, waiting for transfers between devices, per_device(): branch = jnp.sum(lax.all_gather(branch_part, 'ra'), axis=0)  9.22 us
  transfers between devices with their start and end apart: 3, of which 3 were waited for; matrix products, arithmetic and copies ran while one was open for 0% of the time, Pallas kernels for 0%

profile of v1, /device:TPU:0, one launch (start us, length us, event | category | flops | bytes accessed | tf_op | source)
XLA Modules:
  0.0 326.7 jit_solution(1673490704276656736)
XLA Ops:
  6.5 0.0 reduce-scatter.2.cloned.1.call-start
  6.5 1.2 convert_reduce_fusion
  7.7 13.5 %psum.28 = f32[256]{0:T(256)S(1)} all-reduce(f32[256]{0:T(256)S(1)} %convert_reduce_fusion), channel_id=1, replica_groups=mesh['ra'=2,'cb'=4,'dp'=4] {'cb'}, use_global_device_ids=true, to_apply=%region_1.0 | all-reduce | flops 256 | bytes 2048 | tf_op jit(solution)/shard_map/psum | solution.py:9
  21.2 1.3 fusion.2
  22.5 8.4 %psum.29 = f32[256]{0:T(256)S(1)} all-reduce(f32[256]{0:T(256)S(1)} %fusion.2), channel_id=1, replica_groups=mesh['ra'=2,'cb'=4,'dp'=4] {'cb'}, use_global_device_ids=true, to_apply=%region_3.0 | all-reduce | flops 256 | bytes 2048 | tf_op jit(solution)/shard_map/psum | solution.py:12
  30.9 13.8 %fusion.7 = f32[256,8192]{1,0:T(8,128)} fusion(bf16[1024,8192]{1,0:T(8,128)(2,1)} %param.10, bf16[256,1024]{1,0:T(8,128)(2,1)} %param.7, f32[1024]{0:T(1024)} %param.9, f32[1024]{0:T(1024)} %param.8, f32[256]{0:T(256)S(1)} %add_rsqrt_fusion.1, f32[256]{0:T(256)S(1)} %broadcast_multiply_fusion.1), kind=kOutput, calls=%fused_computation.17 | convolution fusion | flops 4296540160 | bytes 25700352 | tf_op jit(solution)/shard_map/dot_general | solution.py:20
  44.8 0.0 reduce-scatter.2.cloned.1.call-update
  44.8 0.0 all-gather.4.cloned.1.call-start
  44.8 144.4 %reduce-scatter.2.cloned.1.call-done = f32[256,2048]{1,0:T(8,128)} async-done(((f32[256,8192]{1,0:T(8,128)}), f32[256,2048]{1,0:T(8,128)}) %reduce-scatter.2.cloned.1.call-update) | async-done | bytes 2097168 | tf_op jit(solution)/shard_map/reduce_scatter | solution.py:21
  189.2 2.8 multiply_convert_fusion
  192.0 0.0 all-gather.4.cloned.1.call-update
  192.0 0.0 copy-start
  192.0 0.0 copy-start.1
  192.1 0.0 copy-start.2
  192.1 0.0 copy-start.3
  192.1 0.0 copy-start.4
  192.1 0.0 all-gather.6.cloned.1.call-start
  192.1 81.4 %all-gather.4.cloned.1.call-done = bf16[256,8192]{1,0:T(8,128)(2,1)} async-done(((bf16[256,2048]{1,0:T(8,128)(2,1)}), bf16[256,8192]{1,0:T(8,128)(2,1)}) %all-gather.4.cloned.1.call-update) | async-done | bytes 4194320 | tf_op jit(solution)/shard_map/all_gather | solution.py:24
  273.5 12.5 %fusion.9 = f32[256,1024]{1,0:T(8,128)} fusion(bf16[256,8192]{1,0:T(8,128)(2,1)} %all-gather.4.cloned.1.call-done, bf16[8192,1024]{1,0:T(8,128)(2,1)} %param.11), kind=kOutput, calls=%fused_computation.18 | convolution fusion | flops 4294967296 | bytes 22020096 | tf_op jit(solution)/shard_map/dot_general | solution.py:23
  286.0 0.0 all-gather.6.cloned.1.call-update
  286.1 9.2 %all-gather.6.cloned.1.call-done = f32[512,1024]{1,0:T(8,128)} async-done(((f32[256,1024]{1,0:T(8,128)}), f32[512,1024]{1,0:T(8,128)}) %all-gather.6.cloned.1.call-update) | async-done | bytes 2097168 | tf_op jit(solution)/shard_map/all_gather | solution.py:28
  295.3 1.9 reduce_sum.47
  297.2 0.0 copy-done
  297.2 0.0 copy-done.1
  297.2 0.0 copy-done.2
  297.2 0.5 fusion.6
  297.7 12.0 %psum.30 = f32[256]{0:T(256)S(1)} all-reduce(f32[256]{0:T(256)S(1)} %fusion.6), channel_id=1, replica_groups=mesh['ra'=2,'cb'=4,'dp'=4] {'cb'}, use_global_device_ids=true, to_apply=%region_7.8 | all-reduce | flops 256 | bytes 2048 | tf_op jit(solution)/shard_map/psum | solution.py:9
  309.6 0.5 multiply_reduce_fusion
  310.2 8.4 %psum.31 = f32[256]{0:T(256)S(1)} all-reduce(f32[256]{0:T(256)S(1)} %multiply_reduce_fusion), channel_id=1, replica_groups=mesh['ra'=2,'cb'=4,'dp'=4] {'cb'}, use_global_device_ids=true, to_apply=%region_9.10 | all-reduce | flops 256 | bytes 2048 | tf_op jit(solution)/shard_map/psum | solution.py:12
  318.6 0.0 copy-done.3
  318.6 0.0 copy-done.4
  318.6 1.6 add_convert_fusion
  (4 shorter events, 0.0 us)
Async XLA Ops:
  6.5 182.7 %reduce-scatter.2.cloned.1.call-start = ((), (), s32[]{:S(2)}) async-start(), calls=%async_computation.1 | async-start | bytes 10485760 | tf_op jit(solution)/shard_map/reduce_scatter | solution.py:21
  44.8 228.8 %all-gather.4.cloned.1.call-start = ((), (), s32[]{:S(2)}) async-start(), calls=%async_computation.2 | async-start | bytes 5242880 | tf_op jit(solution)/shard_map/all_gather | solution.py:24
  192.0 105.1 %copy-start = (bf16[256,1024]{1,0:T(8,128)(2,1)S(1)}, bf16[256,1024]{1,0:T(8,128)(2,1)}, u32[]{:S(2)}) copy-start(bf16[256,1024]{1,0:T(8,128)(2,1)} %param.7) | copy-start | bytes 1572868
  192.0 105.1 %copy-start.1 = (f32[1024]{0:T(1024)S(1)}, f32[1024]{0:T(1024)}, u32[]{:S(2)}) copy-start(f32[1024]{0:T(1024)} %param.9) | copy-start | bytes 12292
  192.1 105.1 %copy-start.2 = (f32[1024]{0:T(1024)S(1)}, f32[1024]{0:T(1024)}, u32[]{:S(2)}) copy-start(f32[1024]{0:T(1024)} %param.8) | copy-start | bytes 12292
  192.1 126.5 %copy-start.3 = (f32[1024]{0:T(1024)S(1)}, f32[1024]{0:T(1024)}, u32[]{:S(2)}) copy-start(f32[1024]{0:T(1024)} %param.13) | copy-start | bytes 12292
  192.1 126.5 %copy-start.4 = (f32[1024]{0:T(1024)S(1)}, f32[1024]{0:T(1024)}, u32[]{:S(2)}) copy-start(f32[1024]{0:T(1024)} %param.12) | copy-start | bytes 12292
  192.1 103.2 %all-gather.6.cloned.1.call-start = ((), (), s32[]{:S(2)}) async-start(), calls=%async_computation.3 | async-start | bytes 3145728 | tf_op jit(solution)/shard_map/all_gather | solution.py:28
Sparse Core Ops, SparseCore 0:
  44.9 144.2 reduce-scatter.1
  192.2 81.3 all-gather.3
  286.2 9.0 all-gather.5
